TPU v7x, 32 devices: a whole 2x2x4 slice. The times are simulated.
32 devices in a mesh: fs: 16 (over z, y, x), tp: 2 (over core).
Axes of the slice: x: 2, y: 2, z: 4, core: 2. Of those that a mesh axis runs over, the one named last changes fastest.
Arguments:
- saved_inputs: bfloat16 [12288, 2048], P('fs'), may hold values from -6 to 6
- cotangents: bfloat16 [3, 12288, 1024], P(None, 'fs', 'tp'), may hold values from -0.0546875 to 0.0546875
- left_roots: float32 [3, 2048, 2048], P(None, 'fs'), may hold values from -1 to 2
- right_roots: float32 [3, 1024, 128], P(None, 'tp'), may hold values from -1 to 2
- moments: float32 [3, 2048, 1024], P(None, 'fs', 'tp'), may hold values from -125 to 125
- masters: float32 [3, 2048, 1024], P(None, 'fs', 'tp'), may hold values from -3 to 3
Outputs:
- direction: float32 [3, 2048, 1024], P(None, 'fs', 'tp')
- moments_new: float32 [3, 2048, 1024], P(None, 'fs', 'tp')
- copies: bfloat16 [3, 2048, 1024], P(None, None, 'tp')
All inputs are finite; a program needn't handle non-finite values.
Results may differ from a plain program's by a relative error of at most 0.002.
Values may be sent and summed in bfloat16 or wider, within the bound.
A program may use at most 64 MiB of HBM per device.

v0:
```python
import jax
import jax.numpy as jnp
from jax import lax
from jax.sharding import PartitionSpec as P

D = 2048
SBW = 1024
RB = 128
momentum_decay = 0.9
step_rate = 0.1
eps_value = 1e-06


def on_device(saved_inputs, cotangents, left_roots, right_roots, moments, masters):
    rows_own = masters.shape[1]
    columns = masters.shape[2]
    grad_rows = lax.psum_scatter(
        jnp.einsum("td,mtc->dmc", saved_inputs, cotangents, preferred_element_type=jnp.float32),
        "fs",
        scatter_dimension=0,
        tiled=True,
    )
    empty = jnp.zeros((3, rows_own, columns), jnp.float32)
    left_done = empty + jnp.einsum(
        "mrn,nmc->mrc",
        left_roots,
        lax.all_gather(grad_rows.astype(jnp.bfloat16), "fs", axis=0, tiled=True).astype(
            jnp.float32
        ),
        precision=lax.Precision.HIGHEST,
    )
    block_count = columns // RB
    right_blocks = right_roots.reshape(3, block_count, RB, RB)
    right_done = jnp.einsum(
        "mrbi,mbij->mrbj",
        left_done.reshape(3, rows_own, block_count, RB),
        right_blocks,
        precision=lax.Precision.HIGHEST,
    ).reshape(3, rows_own, columns)
    moments_new = momentum_decay * moments + right_done
    totals = lax.psum(jnp.sum(moments_new * moments_new, axis=(1, 2)), ("fs", "tp"))
    meansq = totals / (D * SBW)
    direction = moments_new * lax.rsqrt(meansq + eps_value)[:, None, None]
    copy_rows = (masters - step_rate * direction).astype(jnp.bfloat16)
    copies = lax.all_gather(copy_rows, "fs", axis=1, tiled=True)
    return (direction, moments_new, copies)


def solution(mesh):
    placed = (
        P("fs", None),
        P(None, "fs", "tp"),
        P(None, "fs", None),
        P(None, "tp", None),
        P(None, "fs", "tp"),
        P(None, "fs", "tp"),
    )
    return jax.shard_map(
        on_device,
        mesh=mesh,
        in_specs=placed,
        out_specs=(P(None, "fs", "tp"), P(None, "fs", "tp"), P(None, None, "tp")),
        check_vma=False,
    )
```

profile of v0, /device:TPU:0, one launch (start us, length us, event | category | flops | bytes accessed | tf_op | source)
XLA Modules:
  0.0 505.3 jit_solution(11344276064925415366)
XLA Ops:
  7.2 0.0 copy-start
  7.2 0.0 reduce-scatter.2.cloned.1.call-start
  7.2 1.8 copy-done
  9.1 9.7 %fusion = f32[2048,3,512]{0,2,1:T(8,128)} fusion(bf16[3,768,512]{2,1,0:T(8,128)(2,1)} %param.7, bf16[768,2048]{1,0:T(8,128)(2,1)S(1)} %copy-done), kind=kOutput, calls=%fused_computation | convolution fusion | flops 4831838208 | bytes 18087936 | tf_op jit(solution)/shard_map/td,mtc->dmc/dot_general | solution.py:18
  18.7 0.0 reduce-scatter.2.cloned.1.call-update
  18.7 0.0 all-gather.3.cloned.1.call-start
  18.8 205.6 %reduce-scatter.2.cloned.1.call-done = f32[128,3,512]{0,2,1:T(8,128)} async-done(((f32[2048,3,512]{0,2,1:T(8,128)}), f32[128,3,512]{0,2,1:T(8,128)}) %reduce-scatter.2.cloned.1.call-update) | async-done | bytes 786448 | tf_op jit(solution)/shard_map/reduce_scatter | solution.py:17
  224.4 1.9 convert_element_type.7
  226.3 0.0 all-gather.3.cloned.1.call-update
  226.3 0.0 all-gather.5.cloned.1.call-start
  226.4 115.8 %all-gather.3.cloned.1.call-done = bf16[2048,3,512]{0,2,1:T(8,128)(2,1)} async-done(((bf16[128,3,512]{0,2,1:T(8,128)(2,1)}), bf16[2048,3,512]{0,2,1:T(8,128)(2,1)}) %all-gather.3.cloned.1.call-update) | async-done | bytes 6291472 | tf_op jit(solution)/shard_map/all_gather | solution.py:27
  342.2 0.0 copy-start.1
  342.2 8.4 %fusion.2 = f32[3,512,128]{2,1,0:T(8,128)S(1)} fusion(bf16[2048,3,512]{0,2,1:T(8,128)(2,1)} %all-gather.3.cloned.1.call-done, f32[3,128,2048]{2,1,0:T(8,128)} %param.8), kind=kOutput, calls=%fused_computation.7 | convolution fusion | flops 4831838208 | bytes 10223616 | tf_op jit(solution)/shard_map/mrn,nmc->mrc/dot_general | solution.py:24
  350.6 0.0 copy-done.1
  350.6 2.3 fusion.3
  352.9 2.3 copy.11
  355.2 2.4 multiply_reduce_fusion
  357.6 38.3 %psum.7 = f32[3]{0:T(128)S(1)} all-reduce(f32[3]{0:T(128)S(1)} %get-tuple-element.5), channel_id=1, replica_groups=mesh['fs'=16,'tp'=2] {'fs','tp'}, use_global_device_ids=true, to_apply=%region_2.0 | all-reduce | flops 3 | bytes 24 | tf_op jit(solution)/shard_map/psum | solution.py:41
  395.9 2.6 subtract_convert_fusion
  398.5 0.0 all-gather.5.cloned.1.call-update
  398.6 94.3 %all-gather.5.cloned.1.call-done = bf16[3,2048,512]{2,1,0:T(8,128)(2,1)} async-done(((bf16[3,128,512]{2,1,0:T(8,128)(2,1)}), bf16[3,2048,512]{2,1,0:T(8,128)(2,1)}) %all-gather.5.cloned.1.call-update) | async-done | bytes 6291472 | tf_op jit(solution)/shard_map/all_gather | solution.py:45
  492.9 5.9 %copy.15 = bf16[3,2048,512]{2,1,0:T(8,128)(2,1)} copy(bf16[3,2048,512]{2,1,0:T(8,128)(2,1)} %all-gather.5.cloned.1.call-done) | data formatting | bytes 12582912
  (1 shorter events, 0.0 us)
Async XLA Ops:
  7.2 1.9 copy-start
  7.2 217.2 %reduce-scatter.2.cloned.1.call-start = ((), (), s32[]{:S(2)}) async-start(), calls=%async_computation.1 | async-start | bytes 13369344 | tf_op jit(solution)/shard_map/reduce_scatter | solution.py:17
  18.7 323.4 %all-gather.3.cloned.1.call-start = ((), (), s32[]{:S(2)}) async-start(), calls=%async_computation.2 | async-start | bytes 6684672 | tf_op jit(solution)/shard_map/all_gather | solution.py:27
  226.3 266.5 %all-gather.5.cloned.1.call-start = ((), (), s32[]{:S(2)}) async-start(), calls=%async_computation.3 | async-start | bytes 6684672 | tf_op jit(solution)/shard_map/all_gather | solution.py:45
  342.2 8.4 %copy-start.1 = (f32[3,512,128]{2,1,0:T(8,128)S(1)}, f32[3,512,128]{2,1,0:T(8,128)}, u32[]{:S(2)}) copy-start(f32[3,512,128]{2,1,0:T(8,128)} %param.9) | copy-start | bytes 2359300
Sparse Core Ops, SparseCore 0:
  18.9 205.4 reduce-scatter.1
  227.7 114.4 all-gather.2
  398.7 94.1 all-gather.4
where the time goes:
time: 506 us; the launch traced here: 505 us
  waiting for transfers between devices  416 us (82%)
  blocking collectives  38.3 us (8%)
  matrix products  20.4 us (4%)
  between operations  13.8 us (3%)
  local copies, waits for them, and re-layouts  10 us (2%)
  other arithmetic  6.93 us (1%)
    reduce_scatter x1, waiting for transfers between devices, on_device(): lax.psum_scatter(jnp.einsum('td,mtc->dmc', saved_inputs, cotangents, pref...  206 us
    all_gather x1, waiting for transfers between devices, on_device(): lax.all_gather(grad_rows.astype(jnp.bfloat16), 'fs', axis=0, tiled=True)  116 us
    all_gather x1, waiting for transfers between devices, on_device(): copies = lax.all_gather(copy_rows, 'fs', axis=1, tiled=True)  94.3 us
    psum x1, blocking collectives, on_device(): lax.psum(jnp.sum(moments_new * moments_new, axis=(1, 2)), ('fs', 'tp'))  38.3 us
  transfers between devices with their start and end apart: 3, of which 3 were waited for; matrix products, arithmetic and copies ran while one was open for 0% of the time, Pallas kernels for 0%

commit v1 on v0

--- a/solution.py
+++ b/solution.py
@@ -42,7 +42,12 @@
     meansq = totals / (D * SBW)
     direction = moments_new * lax.rsqrt(meansq + eps_value)[:, None, None]
     copy_rows = (masters - step_rate * direction).astype(jnp.bfloat16)
-    copies = lax.all_gather(copy_rows, "fs", axis=1, tiled=True)
+    ring = [copy_rows]
+    for hop in range(15):
+        ring.append(lax.ppermute(ring[-1], "fs", [(dev, (dev + 1) % 16) for dev in range(16)]))
+    copies = jnp.roll(
+        jnp.concatenate(ring[::-1], axis=1), (lax.axis_index("fs") + 1) * ring[0].shape[1], axis=1
+    )
     return (direction, moments_new, copies)
 
 

time: 506 us -> 630 us (1.25)
  waiting for transfers between devices: 416 us -> 511 us
  local copies, waits for them, and re-layouts: 10 us -> 34.9 us
    ppermute x0 -> x15, waiting for transfers between devices: none -> 190 us  [on_device(): lax.ppermute(ring[-1], 'fs', [(dev, (dev + 1) % 16) for dev in range(16)])]
    all_gather x1 -> x0, waiting for transfers between devices: 94.3 us -> none  [on_device(): copies = lax.all_gather(copy_rows, 'fs', axis=1, tiled=True)]
    unnamed x5 -> x87, local copies, waits for them, and re-layouts: 7.74 us -> 29.5 us
  transfers between devices with their start and end apart: 3 -> 17, of which waited for: 3 -> 17; matrix products, arithmetic and copies ran while one was open for 0% -> 0% of each run, Pallas kernels for 0% -> 0%
where the time goes in v1:
time: 630 us; the launch traced here: 629 us
  waiting for transfers between devices  511 us (81%)
  blocking collectives  38.3 us (6%)
  local copies, waits for them, and re-layouts  34.9 us (6%)
  matrix products  20.4 us (3%)
  between operations  14.5 us (2%)
  other arithmetic  6.81 us (1%)
    reduce_scatter x1, waiting for transfers between devices, on_device(): lax.psum_scatter(jnp.einsum('td,mtc->dmc', saved_inputs, cotangents, pref...  206 us
    ppermute x15, waiting for transfers between devices, on_device(): lax.ppermute(ring[-1], 'fs', [(dev, (dev + 1) % 16) for dev in range(16)])  190 us
    all_gather x1, waiting for transfers between devices, on_device(): lax.all_gather(grad_rows.astype(jnp.bfloat16), 'fs', axis=0, tiled=True)  116 us
    psum x1, blocking collectives, on_device(): lax.psum(jnp.sum(moments_new * moments_new, axis=(1, 2)), ('fs', 'tp'))  38.3 us
    unnamed x87, local copies, waits for them, and re-layouts  29.5 us
  transfers between devices with their start and end apart: 17, of which 17 were waited for; matrix products, arithmetic and copies ran while one was open for 0% of the time, Pallas kernels for 0%

profile of v1, /device:TPU:0, one launch (start us, length us, event | category | flops | bytes accessed | tf_op | source)
XLA Modules:
  0.0 628.6 jit_solution(2265179701594666167)
XLA Ops:
  7.2 1.8 copy-done
  9.1 9.7 %fusion = f32[2048,3,512]{0,2,1:T(8,128)} fusion(bf16[3,768,512]{2,1,0:T(8,128)(2,1)} %param.7, bf16[768,2048]{1,0:T(8,128)(2,1)S(1)} %copy-done), kind=kOutput, calls=%fused_computation | convolution fusion | flops 4831838208 | bytes 18087936 | tf_op jit(solution)/shard_map/td,mtc->dmc/dot_general | solution.py:18
  18.8 205.6 %reduce-scatter.2.cloned.1.call-done = f32[128,3,512]{0,2,1:T(8,128)} async-done(((f32[2048,3,512]{0,2,1:T(8,128)}), f32[128,3,512]{0,2,1:T(8,128)}) %reduce-scatter.2.cloned.1.call-update) | async-done | bytes 786448 | tf_op jit(solution)/shard_map/reduce_scatter | solution.py:17
  224.4 1.9 convert_element_type.7
  226.3 115.8 %all-gather.2.cloned.1.call-done = bf16[2048,3,512]{0,2,1:T(8,128)(2,1)} async-done(((bf16[128,3,512]{0,2,1:T(8,128)(2,1)}), bf16[2048,3,512]{0,2,1:T(8,128)(2,1)}) %all-gather.2.cloned.1.call-update) | async-done | bytes 6291472 | tf_op jit(solution)/shard_map/all_gather | solution.py:27
  342.2 8.4 %fusion.2 = f32[3,512,128]{2,1,0:T(8,128)S(1)} fusion(bf16[2048,3,512]{0,2,1:T(8,128)(2,1)} %all-gather.2.cloned.1.call-done, f32[3,128,2048]{2,1,0:T(8,128)} %param.8), kind=kOutput, calls=%fused_computation.40 | convolution fusion | flops 4831838208 | bytes 10223616 | tf_op jit(solution)/shard_map/mrn,nmc->mrc/dot_general | solution.py:24
  350.6 2.3 fusion.3
  352.9 2.3 copy.11
  355.2 2.4 multiply_reduce_fusion
  357.6 38.3 %psum.7 = f32[3]{0:T(128)S(1)} all-reduce(f32[3]{0:T(128)S(1)} %get-tuple-element.5), channel_id=1, replica_groups=mesh['fs'=16,'tp'=2] {'fs','tp'}, use_global_device_ids=true, to_apply=%region_2.0 | all-reduce | flops 3 | bytes 24 | tf_op jit(solution)/shard_map/psum | solution.py:41
  395.9 2.5 subtract_convert_fusion
  398.4 2.3 collective-permute-start
  400.7 11.4 %collective-permute-done = bf16[3,128,512]{2,1,0:T(8,128)(2,1)S(1)} collective-permute-done((bf16[3,128,512]{2,1,0:T(8,128)(2,1)S(1)}, bf16[3,128,512]{2,1,0:T(8,128)(2,1)S(1)}, u32[]{:S(2)}, u32[]{:S(2)}) %collective-permute-start) | collective-permute-done | bytes 393248 | tf_op jit(solution)/shard_map/ppermute | solution.py:47
  412.8 12.8 %collective-permute-done.1 = bf16[3,128,512]{2,1,0:T(8,128)(2,1)S(1)} collective-permute-done((bf16[3,128,512]{2,1,0:T(8,128)(2,1)S(1)}, bf16[3,128,512]{2,1,0:T(8,128)(2,1)S(1)}, u32[]{:S(2)}, u32[]{:S(2)}) %collective-permute-start.1) | collective-permute-done | bytes 393248 | tf_op jit(solution)/shard_map/ppermute | solution.py:47
  426.3 11.9 %collective-permute-done.2 = bf16[3,128,512]{2,1,0:T(8,128)(2,1)S(1)} collective-permute-done((bf16[3,128,512]{2,1,0:T(8,128)(2,1)S(1)}, bf16[3,128,512]{2,1,0:T(8,128)(2,1)S(1)}, u32[]{:S(2)}, u32[]{:S(2)}) %collective-permute-start.2) | collective-permute-done | bytes 393248 | tf_op jit(solution)/shard_map/ppermute | solution.py:47
  439.0 11.4 %collective-permute-done.3 = bf16[3,128,512]{2,1,0:T(8,128)(2,1)S(1)} collective-permute-done((bf16[3,128,512]{2,1,0:T(8,128)(2,1)S(1)}, bf16[3,128,512]{2,1,0:T(8,128)(2,1)S(1)}, u32[]{:S(2)}, u32[]{:S(2)}) %collective-permute-start.3) | collective-permute-done | bytes 393248 | tf_op jit(solution)/shard_map/ppermute | solution.py:47
  450.4 0.8 copy-done.7
  451.2 11.4 %collective-permute-done.4 = bf16[3,128,512]{2,1,0:T(8,128)(2,1)S(1)} collective-permute-done((bf16[3,128,512]{2,1,0:T(8,128)(2,1)S(1)}, bf16[3,128,512]{2,1,0:T(8,128)(2,1)S(1)}, u32[]{:S(2)}, u32[]{:S(2)}) %collective-permute-start.4) | collective-permute-done | bytes 393248 | tf_op jit(solution)/shard_map/ppermute | solution.py:47
  463.3 11.4 %collective-permute-done.5 = bf16[3,128,512]{2,1,0:T(8,128)(2,1)S(1)} collective-permute-done((bf16[3,128,512]{2,1,0:T(8,128)(2,1)S(1)}, bf16[3,128,512]{2,1,0:T(8,128)(2,1)S(1)}, u32[]{:S(2)}, u32[]{:S(2)}) %collective-permute-start.5) | collective-permute-done | bytes 393248 | tf_op jit(solution)/shard_map/ppermute | solution.py:47
  475.5 12.6 %collective-permute-done.6 = bf16[3,128,512]{2,1,0:T(8,128)(2,1)S(1)} collective-permute-done((bf16[3,128,512]{2,1,0:T(8,128)(2,1)S(1)}, bf16[3,128,512]{2,1,0:T(8,128)(2,1)S(1)}, u32[]{:S(2)}, u32[]{:S(2)}) %collective-permute-start.6) | collective-permute-done | bytes 393248 | tf_op jit(solution)/shard_map/ppermute | solution.py:47
  488.0 0.8 copy-done.13
  488.8 13.7 %collective-permute-done.7 = bf16[3,128,512]{2,1,0:T(8,128)(2,1)S(1)} collective-permute-done((bf16[3,128,512]{2,1,0:T(8,128)(2,1)S(1)}, bf16[3,128,512]{2,1,0:T(8,128)(2,1)S(1)}, u32[]{:S(2)}, u32[]{:S(2)}) %collective-permute-start.7) | collective-permute-done | bytes 393248 | tf_op jit(solution)/shard_map/ppermute | solution.py:47
  502.5 0.8 copy-done.15
  503.2 14.9 %collective-permute-done.8 = bf16[3,128,512]{2,1,0:T(8,128)(2,1)S(1)} collective-permute-done((bf16[3,128,512]{2,1,0:T(8,128)(2,1)S(1)}, bf16[3,128,512]{2,1,0:T(8,128)(2,1)S(1)}, u32[]{:S(2)}, u32[]{:S(2)}) %collective-permute-start.8) | collective-permute-done | bytes 393248 | tf_op jit(solution)/shard_map/ppermute | solution.py:47
  518.9 15.1 %collective-permute-done.9 = bf16[3,128,512]{2,1,0:T(8,128)(2,1)S(1)} collective-permute-done((bf16[3,128,512]{2,1,0:T(8,128)(2,1)S(1)}, bf16[3,128,512]{2,1,0:T(8,128)(2,1)S(1)}, u32[]{:S(2)}, u32[]{:S(2)}) %collective-permute-start.9) | collective-permute-done | bytes 393248 | tf_op jit(solution)/shard_map/ppermute | solution.py:47
  534.7 14.3 %collective-permute-done.10 = bf16[3,128,512]{2,1,0:T(8,128)(2,1)S(1)} collective-permute-done((bf16[3,128,512]{2,1,0:T(8,128)(2,1)S(1)}, bf16[3,128,512]{2,1,0:T(8,128)(2,1)S(1)}, u32[]{:S(2)}, u32[]{:S(2)}) %collective-permute-start.10) | collective-permute-done | bytes 393248 | tf_op jit(solution)/shard_map/ppermute | solution.py:47
  549.8 13.4 %collective-permute-done.11 = bf16[3,128,512]{2,1,0:T(8,128)(2,1)S(1)} collective-permute-done((bf16[3,128,512]{2,1,0:T(8,128)(2,1)S(1)}, bf16[3,128,512]{2,1,0:T(8,128)(2,1)S(1)}, u32[]{:S(2)}, u32[]{:S(2)}) %collective-permute-start.11) | collective-permute-done | bytes 393248 | tf_op jit(solution)/shard_map/ppermute | solution.py:47
  564.0 12.6 %collective-permute-done.12 = bf16[3,128,512]{2,1,0:T(8,128)(2,1)S(1)} collective-permute-done((bf16[3,128,512]{2,1,0:T(8,128)(2,1)S(1)}, bf16[3,128,512]{2,1,0:T(8,128)(2,1)S(1)}, u32[]{:S(2)}, u32[]{:S(2)}) %collective-permute-start.12) | collective-permute-done | bytes 393248 | tf_op jit(solution)/shard_map/ppermute | solution.py:47
  577.3 11.5 %collective-permute-done.13 = bf16[3,128,512]{2,1,0:T(8,128)(2,1)} collective-permute-done((bf16[3,128,512]{2,1,0:T(8,128)(2,1)S(1)}, bf16[3,128,512]{2,1,0:T(8,128)(2,1)}, u32[]{:S(2)}, u32[]{:S(2)}) %collective-permute-start.13) | collective-permute-done | bytes 393248 | tf_op jit(solution)/shard_map/ppermute | solution.py:47
  588.9 11.6 %collective-permute-done.14 = bf16[3,128,512]{2,1,0:T(8,128)(2,1)} collective-permute-done((bf16[3,128,512]{2,1,0:T(8,128)(2,1)}, bf16[3,128,512]{2,1,0:T(8,128)(2,1)}, u32[]{:S(2)}, u32[]{:S(2)}) %collective-permute-start.14) | collective-permute-done | bytes 393248 | tf_op jit(solution)/shard_map/ppermute | solution.py:47
  600.5 1.0 constant_dynamic-update-slice_fusion.31
  601.5 1.0 constant_dynamic-update-slice_fusion.30
  602.6 1.0 constant_dynamic-update-slice_fusion.29
  603.6 1.0 constant_dynamic-update-slice_fusion.28
  604.6 1.0 constant_dynamic-update-slice_fusion.27
  605.6 1.0 constant_dynamic-update-slice_fusion.26
  606.7 1.0 constant_dynamic-update-slice_fusion.25
  607.7 1.0 constant_dynamic-update-slice_fusion.24
  608.7 1.0 constant_dynamic-update-slice_fusion.23
  609.7 1.0 constant_dynamic-update-slice_fusion.22
  610.8 1.0 constant_dynamic-update-slice_fusion.21
  611.8 1.0 constant_dynamic-update-slice_fusion.20
  612.8 1.0 constant_dynamic-update-slice_fusion.19
  613.8 1.0 constant_dynamic-update-slice_fusion.18
  614.9 1.0 constant_dynamic-update-slice_fusion.17
  615.9 1.0 constant_dynamic-update-slice_fusion.15
  617.0 1.0 constant_dynamic-update-slice_fusion.14
  618.6 3.1 constant_dynamic-slice_fusion
  (86 shorter events, 8.1 us)
Async XLA Ops:
  7.2 1.9 copy-start
  7.2 217.2 %reduce-scatter.2.cloned.1.call-start = ((), (), s32[]{:S(2)}) async-start(), calls=%async_computation.1 | async-start | bytes 13369344 | tf_op jit(solution)/shard_map/reduce_scatter | solution.py:17
  18.7 323.4 %all-gather.2.cloned.1.call-start = ((), (), s32[]{:S(2)}) async-start(), calls=%async_computation.2 | async-start | bytes 6684672 | tf_op jit(solution)/shard_map/all_gather | solution.py:27
  342.2 8.4 %copy-start.27 = (f32[3,512,128]{2,1,0:T(8,128)S(1)}, f32[3,512,128]{2,1,0:T(8,128)}, u32[]{:S(2)}) copy-start(f32[3,512,128]{2,1,0:T(8,128)} %param.9) | copy-start | bytes 2359300
  398.4 13.6 %collective-permute-start = (bf16[3,128,512]{2,1,0:T(8,128)(2,1)S(1)}, bf16[3,128,512]{2,1,0:T(8,128)(2,1)S(1)}, u32[]{:S(2)}, u32[]{:S(2)}) collective-permute-start(bf16[3,128,512]{2,1,0:T(8,128)(2,1)S(1)} %get-tuple-element.3), channel_id=1, source_target_pairs={{0,2},{2,4},{4,6},{6,8},{8,10},{10,12},{12,14},{14,16},{16,18},{18... | collective-permute-start | bytes 1179656 | tf_op jit(solution)/shard_map/ppermute | solution.py:47
  412.1 0.7 copy-start.1
  412.8 12.8 %collective-permute-start.1 = (bf16[3,128,512]{2,1,0:T(8,128)(2,1)S(1)}, bf16[3,128,512]{2,1,0:T(8,128)(2,1)S(1)}, u32[]{:S(2)}, u32[]{:S(2)}) collective-permute-start(bf16[3,128,512]{2,1,0:T(8,128)(2,1)S(1)} %collective-permute-done), channel_id=1, source_target_pairs={{0,2},{2,4},{4,6},{6,8},{8,10},{10,12},{12,14},{14,16},{16,18},{18... | collective-permute-start | bytes 1179656 | tf_op jit(solution)/shard_map/ppermute | solution.py:47
  425.6 0.8 copy-start.3
  426.3 11.9 %collective-permute-start.2 = (bf16[3,128,512]{2,1,0:T(8,128)(2,1)S(1)}, bf16[3,128,512]{2,1,0:T(8,128)(2,1)S(1)}, u32[]{:S(2)}, u32[]{:S(2)}) collective-permute-start(bf16[3,128,512]{2,1,0:T(8,128)(2,1)S(1)} %collective-permute-done.1), channel_id=1, source_target_pairs={{0,2},{2,4},{4,6},{6,8},{8,10},{10,12},{12,14},{14,16},{16,18},{18... | collective-permute-start | bytes 1179656 | tf_op jit(solution)/shard_map/ppermute | solution.py:47
  438.3 0.7 copy-start.5
  439.0 11.4 %collective-permute-start.3 = (bf16[3,128,512]{2,1,0:T(8,128)(2,1)S(1)}, bf16[3,128,512]{2,1,0:T(8,128)(2,1)S(1)}, u32[]{:S(2)}, u32[]{:S(2)}) collective-permute-start(bf16[3,128,512]{2,1,0:T(8,128)(2,1)S(1)} %collective-permute-done.2), channel_id=1, source_target_pairs={{0,2},{2,4},{4,6},{6,8},{8,10},{10,12},{12,14},{14,16},{16,18},{18... | collective-permute-start | bytes 1179656 | tf_op jit(solution)/shard_map/ppermute | solution.py:47
  450.4 0.8 copy-start.7
  451.2 11.4 %collective-permute-start.4 = (bf16[3,128,512]{2,1,0:T(8,128)(2,1)S(1)}, bf16[3,128,512]{2,1,0:T(8,128)(2,1)S(1)}, u32[]{:S(2)}, u32[]{:S(2)}) collective-permute-start(bf16[3,128,512]{2,1,0:T(8,128)(2,1)S(1)} %collective-permute-done.3), channel_id=1, source_target_pairs={{0,2},{2,4},{4,6},{6,8},{8,10},{10,12},{12,14},{14,16},{16,18},{18... | collective-permute-start | bytes 1179656 | tf_op jit(solution)/shard_map/ppermute | solution.py:47
  462.5 0.8 copy-start.9
  463.3 11.4 %collective-permute-start.5 = (bf16[3,128,512]{2,1,0:T(8,128)(2,1)S(1)}, bf16[3,128,512]{2,1,0:T(8,128)(2,1)S(1)}, u32[]{:S(2)}, u32[]{:S(2)}) collective-permute-start(bf16[3,128,512]{2,1,0:T(8,128)(2,1)S(1)} %collective-permute-done.4), channel_id=1, source_target_pairs={{0,2},{2,4},{4,6},{6,8},{8,10},{10,12},{12,14},{14,16},{16,18},{18... | collective-permute-start | bytes 1179656 | tf_op jit(solution)/shard_map/ppermute | solution.py:47
  474.7 0.8 copy-start.11
  475.5 12.6 %collective-permute-start.6 = (bf16[3,128,512]{2,1,0:T(8,128)(2,1)S(1)}, bf16[3,128,512]{2,1,0:T(8,128)(2,1)S(1)}, u32[]{:S(2)}, u32[]{:S(2)}) collective-permute-start(bf16[3,128,512]{2,1,0:T(8,128)(2,1)S(1)} %collective-permute-done.5), channel_id=1, source_target_pairs={{0,2},{2,4},{4,6},{6,8},{8,10},{10,12},{12,14},{14,16},{16,18},{18... | collective-permute-start | bytes 1179656 | tf_op jit(solution)/shard_map/ppermute | solution.py:47
  488.0 0.8 copy-start.13
  488.8 13.7 %collective-permute-start.7 = (bf16[3,128,512]{2,1,0:T(8,128)(2,1)S(1)}, bf16[3,128,512]{2,1,0:T(8,128)(2,1)S(1)}, u32[]{:S(2)}, u32[]{:S(2)}) collective-permute-start(bf16[3,128,512]{2,1,0:T(8,128)(2,1)S(1)} %collective-permute-done.6), channel_id=1, source_target_pairs={{0,2},{2,4},{4,6},{6,8},{8,10},{10,12},{12,14},{14,16},{16,18},{18... | collective-permute-start | bytes 1179656 | tf_op jit(solution)/shard_map/ppermute | solution.py:47
  502.5 0.8 copy-start.15
  503.2 14.9 %collective-permute-start.8 = (bf16[3,128,512]{2,1,0:T(8,128)(2,1)S(1)}, bf16[3,128,512]{2,1,0:T(8,128)(2,1)S(1)}, u32[]{:S(2)}, u32[]{:S(2)}) collective-permute-start(bf16[3,128,512]{2,1,0:T(8,128)(2,1)S(1)} %collective-permute-done.7), channel_id=1, source_target_pairs={{0,2},{2,4},{4,6},{6,8},{8,10},{10,12},{12,14},{14,16},{16,18},{18... | collective-permute-start | bytes 1179656 | tf_op jit(solution)/shard_map/ppermute | solution.py:47
  518.1 0.8 copy-start.17
  518.8 15.1 %collective-permute-start.9 = (bf16[3,128,512]{2,1,0:T(8,128)(2,1)S(1)}, bf16[3,128,512]{2,1,0:T(8,128)(2,1)S(1)}, u32[]{:S(2)}, u32[]{:S(2)}) collective-permute-start(bf16[3,128,512]{2,1,0:T(8,128)(2,1)S(1)} %collective-permute-done.8), channel_id=1, source_target_pairs={{0,2},{2,4},{4,6},{6,8},{8,10},{10,12},{12,14},{14,16},{16,18},{18... | collective-permute-start | bytes 1179656 | tf_op jit(solution)/shard_map/ppermute | solution.py:47
  534.0 0.7 copy-start.19
  534.7 14.3 %collective-permute-start.10 = (bf16[3,128,512]{2,1,0:T(8,128)(2,1)S(1)}, bf16[3,128,512]{2,1,0:T(8,128)(2,1)S(1)}, u32[]{:S(2)}, u32[]{:S(2)}) collective-permute-start(bf16[3,128,512]{2,1,0:T(8,128)(2,1)S(1)} %collective-permute-done.9), channel_id=1, source_target_pairs={{0,2},{2,4},{4,6},{6,8},{8,10},{10,12},{12,14},{14,16},{16,18},{18... | collective-permute-start | bytes 1179656 | tf_op jit(solution)/shard_map/ppermute | solution.py:47
  549.0 0.8 copy-start.21
  549.8 13.5 %collective-permute-start.11 = (bf16[3,128,512]{2,1,0:T(8,128)(2,1)S(1)}, bf16[3,128,512]{2,1,0:T(8,128)(2,1)S(1)}, u32[]{:S(2)}, u32[]{:S(2)}) collective-permute-start(bf16[3,128,512]{2,1,0:T(8,128)(2,1)S(1)} %collective-permute-done.10), channel_id=1, source_target_pairs={{0,2},{2,4},{4,6},{6,8},{8,10},{10,12},{12,14},{14,16},{16,18},{18... | collective-permute-start | bytes 1179656 | tf_op jit(solution)/shard_map/ppermute | solution.py:47
  563.2 0.8 copy-start.23
  564.0 12.6 %collective-permute-start.12 = (bf16[3,128,512]{2,1,0:T(8,128)(2,1)S(1)}, bf16[3,128,512]{2,1,0:T(8,128)(2,1)S(1)}, u32[]{:S(2)}, u32[]{:S(2)}) collective-permute-start(bf16[3,128,512]{2,1,0:T(8,128)(2,1)S(1)} %collective-permute-done.11), channel_id=1, source_target_pairs={{0,2},{2,4},{4,6},{6,8},{8,10},{10,12},{12,14},{14,16},{16,18},{18... | collective-permute-start | bytes 1179656 | tf_op jit(solution)/shard_map/ppermute | solution.py:47
  576.6 0.7 copy-start.25
  577.3 11.5 %collective-permute-start.13 = (bf16[3,128,512]{2,1,0:T(8,128)(2,1)S(1)}, bf16[3,128,512]{2,1,0:T(8,128)(2,1)}, u32[]{:S(2)}, u32[]{:S(2)}) collective-permute-start(bf16[3,128,512]{2,1,0:T(8,128)(2,1)S(1)} %collective-permute-done.12), channel_id=1, source_target_pairs={{0,2},{2,4},{4,6},{6,8},{8,10},{10,12},{12,14},{14,16},{16,18},{18... | collective-permute-start | bytes 1179656 | tf_op jit(solution)/shard_map/ppermute | solution.py:47
  588.8 11.7 %collective-permute-start.14 = (bf16[3,128,512]{2,1,0:T(8,128)(2,1)}, bf16[3,128,512]{2,1,0:T(8,128)(2,1)}, u32[]{:S(2)}, u32[]{:S(2)}) collective-permute-start(bf16[3,128,512]{2,1,0:T(8,128)(2,1)} %collective-permute-done.13), channel_id=1, source_target_pairs={{0,2},{2,4},{4,6},{6,8},{8,10},{10,12},{12,14},{14,16},{16,18},{18... | collective-permute-start | bytes 1179656 | tf_op jit(solution)/shard_map/ppermute | solution.py:47
  588.8 29.2 %copy-start.26 = (bf16[3,128,512]{2,1,0:T(8,128)(2,1)S(1)}, bf16[3,128,512]{2,1,0:T(8,128)(2,1)}, u32[]{:S(2)}) copy-start(bf16[3,128,512]{2,1,0:T(8,128)(2,1)} %copy-done.25) | copy-start | bytes 1179652
  588.8 29.2 %copy-start.24 = (bf16[3,128,512]{2,1,0:T(8,128)(2,1)S(1)}, bf16[3,128,512]{2,1,0:T(8,128)(2,1)}, u32[]{:S(2)}) copy-start(bf16[3,128,512]{2,1,0:T(8,128)(2,1)} %copy-done.23) | copy-start | bytes 1179652
  588.8 29.3 %copy-start.22 = (bf16[3,128,512]{2,1,0:T(8,128)(2,1)S(1)}, bf16[3,128,512]{2,1,0:T(8,128)(2,1)}, u32[]{:S(2)}) copy-start(bf16[3,128,512]{2,1,0:T(8,128)(2,1)} %copy-done.21) | copy-start | bytes 1179652
  588.8 29.3 %copy-start.20 = (bf16[3,128,512]{2,1,0:T(8,128)(2,1)S(1)}, bf16[3,128,512]{2,1,0:T(8,128)(2,1)}, u32[]{:S(2)}) copy-start(bf16[3,128,512]{2,1,0:T(8,128)(2,1)} %copy-done.19) | copy-start | bytes 1179652
  588.8 29.3 %copy-start.18 = (bf16[3,128,512]{2,1,0:T(8,128)(2,1)S(1)}, bf16[3,128,512]{2,1,0:T(8,128)(2,1)}, u32[]{:S(2)}) copy-start(bf16[3,128,512]{2,1,0:T(8,128)(2,1)} %copy-done.17) | copy-start | bytes 1179652
  588.8 29.4 %copy-start.16 = (bf16[3,128,512]{2,1,0:T(8,128)(2,1)S(1)}, bf16[3,128,512]{2,1,0:T(8,128)(2,1)}, u32[]{:S(2)}) copy-start(bf16[3,128,512]{2,1,0:T(8,128)(2,1)} %copy-done.15) | copy-start | bytes 1179652
  588.9 29.4 %copy-start.14 = (bf16[3,128,512]{2,1,0:T(8,128)(2,1)S(1)}, bf16[3,128,512]{2,1,0:T(8,128)(2,1)}, u32[]{:S(2)}) copy-start(bf16[3,128,512]{2,1,0:T(8,128)(2,1)} %copy-done.13) | copy-start | bytes 1179652
  588.9 29.4 %copy-start.12 = (bf16[3,128,512]{2,1,0:T(8,128)(2,1)S(1)}, bf16[3,128,512]{2,1,0:T(8,128)(2,1)}, u32[]{:S(2)}) copy-start(bf16[3,128,512]{2,1,0:T(8,128)(2,1)} %copy-done.11) | copy-start | bytes 1179652
  588.9 29.5 %copy-start.10 = (bf16[3,128,512]{2,1,0:T(8,128)(2,1)S(1)}, bf16[3,128,512]{2,1,0:T(8,128)(2,1)}, u32[]{:S(2)}) copy-start(bf16[3,128,512]{2,1,0:T(8,128)(2,1)} %copy-done.9) | copy-start | bytes 1179652
  588.9 29.5 %copy-start.8 = (bf16[3,128,512]{2,1,0:T(8,128)(2,1)S(1)}, bf16[3,128,512]{2,1,0:T(8,128)(2,1)}, u32[]{:S(2)}) copy-start(bf16[3,128,512]{2,1,0:T(8,128)(2,1)} %copy-done.7) | copy-start | bytes 1179652
  588.9 29.5 %copy-start.6 = (bf16[3,128,512]{2,1,0:T(8,128)(2,1)S(1)}, bf16[3,128,512]{2,1,0:T(8,128)(2,1)}, u32[]{:S(2)}) copy-start(bf16[3,128,512]{2,1,0:T(8,128)(2,1)} %copy-done.5) | copy-start | bytes 1179652
  588.9 29.6 %copy-start.4 = (bf16[3,128,512]{2,1,0:T(8,128)(2,1)S(1)}, bf16[3,128,512]{2,1,0:T(8,128)(2,1)}, u32[]{:S(2)}) copy-start(bf16[3,128,512]{2,1,0:T(8,128)(2,1)} %copy-done.3) | copy-start | bytes 1179652
  588.9 29.6 %copy-start.2 = (bf16[3,128,512]{2,1,0:T(8,128)(2,1)S(1)}, bf16[3,128,512]{2,1,0:T(8,128)(2,1)}, u32[]{:S(2)}) copy-start(bf16[3,128,512]{2,1,0:T(8,128)(2,1)} %copy-done.1) | copy-start | bytes 1179652
Sparse Core Ops, SparseCore 0:
  18.9 205.4 reduce-scatter.1
  227.7 114.4 all-gather.1
